TPU v7x, 32 devices: a whole 2x2x4 slice. The times are simulated.
32 devices in a mesh: sp: 16 (over z, y, x), tp: 2 (over core).
Axes of the slice: x: 2, y: 2, z: 4, core: 2. Of those that a mesh axis runs over, the one named last changes fastest.
Arguments:
- tokens: bfloat16 [6144, 2048], P('sp', 'tp'), may hold values from -6 to 6
- input_gain: float32 [2048], replicated, may hold values from 0.1 to 1.9
- query_weight: bfloat16 [2048, 1024], P(None, 'tp'), may hold values from -0.5 to 0.5
- query_rot_weight: bfloat16 [2048, 512], P(None, 'tp'), may hold values from -0.125 to 0.125
- kv_down: bfloat16 [2048, 256], replicated, may hold values from -0.5 to 0.5
- rot_down: bfloat16 [2048, 32], replicated, may hold values from -0.125 to 0.125
- kv_gain: float32 [256], replicated, may hold values from 0.1 to 1.9
- key_up: bfloat16 [256, 1024], P(None, 'tp'), may hold values from -0.5 to 0.5
- value_up: bfloat16 [256, 1024], P(None, 'tp'), may hold values from -4 to 4
- conv_value_weight: bfloat16 [2048, 1024], P(None, 'tp'), may hold values from -0.125 to 0.125
- conv_gate_weight: bfloat16 [2048, 1024], P(None, 'tp'), may hold values from -0.125 to 0.125
- conv_taps: float32 [31, 1024], P(None, 'tp'), may hold values from -8 to 8
- conv_ln_gain: float32 [1024], P('tp'), may hold values from 0.1 to 1.9
- conv_ln_bias: float32 [1024], P('tp'), may hold values from -3 to 3
- att_out_gain: float32 [1024], P('tp'), may hold values from 0.1 to 1.9
- conv_out_gain: float32 [1024], P('tp'), may hold values from 0.1 to 1.9
- att_out_weight: bfloat16 [1024, 2048], P('tp'), may hold values from -0.125 to 0.125
- conv_out_weight: bfloat16 [1024, 2048], P('tp'), may hold values from -0.125 to 0.125
Outputs:
- mixed: bfloat16 [6144, 2048], P('sp', 'tp')
All inputs are finite; a program needn't handle non-finite values.
Results may differ from a plain program's by a relative error of at most 0.017.
Values may be sent and summed in bfloat16 or wider, within the bound.
No kernel may reach another device: no remote copies, remote signals or barrier semaphores. Data moves between devices by JAX's collectives and lax.ppermute only.
A program may use at most 128 MiB of HBM per device.

v0:
```python
import math
import jax
import jax.numpy as jnp
from jax import lax
from jax.sharding import PartitionSpec as P

D_MODEL = 2048
NOPE_DIM = 64
ROT_DIM = 32
VALUE_DIM = 64
CONV_CH = 1024
KERNEL = 31
ATT_WIDTH = 1024
norm_eps = 1e-06
far_below = -1e30
rope_base = 10000.0


def shifted(block, axis, distance):
    devices = range(lax.axis_size(axis))
    route = [(i - distance, i) for i in devices if i - distance in devices]
    return lax.ppermute(block, axis, route)


def rotary_tables(positions, half_dim):
    frequency = rope_base ** (-jnp.arange(half_dim, dtype=jnp.float32) / half_dim)
    angles = positions.astype(jnp.float32)[:, None] * frequency[None, :]
    return (jnp.cos(angles), jnp.sin(angles))


def rotate_half(values, cos_table, sine_table):
    half_dim = cos_table.shape[-1]
    front_half = values[..., :half_dim]
    back_half = values[..., half_dim:]
    return jnp.concatenate(
        [
            front_half * cos_table - back_half * sine_table,
            back_half * cos_table + front_half * sine_table,
        ],
        axis=-1,
    )


def shards(
    tokens,
    input_gain,
    query_weight,
    query_rot_weight,
    kv_down,
    rot_down,
    kv_gain,
    key_up,
    value_up,
    conv_value_weight,
    conv_gate_weight,
    conv_taps,
    conv_ln_gain,
    conv_ln_bias,
    att_out_gain,
    conv_out_gain,
    att_out_weight,
    conv_out_weight,
):
    tok_rows = tokens.shape[0]
    heads_here = key_up.shape[1] // NOPE_DIM
    chan_here = conv_taps.shape[1]
    weight_list = (
        query_weight,
        query_rot_weight,
        kv_down,
        rot_down,
        conv_value_weight,
        conv_gate_weight,
    )
    wide_part = lax.all_gather(tokens, "tp", axis=1, tiled=True).astype(jnp.float32)
    scaled = (wide_part * input_gain[None, :]).astype(jnp.bfloat16)

    def add_product(weight):
        return jnp.dot(scaled, weight, preferred_element_type=jnp.float32)

    summed = tuple((add_product(weight) for weight in weight_list))
    q_acc, qrot_acc, latent_raw, rot_acc, value_acc, gate_acc, square_sum = summed + (
        jnp.sum(wide_part * wide_part, axis=1),
    )
    row_scale = lax.rsqrt(square_sum / D_MODEL + norm_eps)[:, None]
    positions = lax.axis_index("sp") * tok_rows + jnp.arange(tok_rows, dtype=jnp.int32)
    cos_table, sine_table = rotary_tables(positions, ROT_DIM // 2)
    queries = (q_acc * row_scale).astype(jnp.bfloat16).reshape(tok_rows, heads_here, NOPE_DIM)
    query_rot = rotate_half(
        (qrot_acc * row_scale).reshape(tok_rows, heads_here, ROT_DIM),
        cos_table[:, None, :],
        sine_table[:, None, :],
    ).astype(jnp.bfloat16)
    latent = (
        latent_raw
        * lax.rsqrt(jnp.mean(latent_raw * latent_raw, axis=1, keepdims=True) + norm_eps)
        * kv_gain[None, :]
    ).astype(jnp.bfloat16)
    key_rot = rotate_half(rot_acc * row_scale, cos_table, sine_table).astype(jnp.bfloat16)
    gated_input = (value_acc * row_scale * jax.nn.sigmoid(gate_acc * row_scale)).astype(
        jnp.bfloat16
    )
    query_end = (lax.axis_index("sp") + 1) * tok_rows
    inv_scale = 1.0 / math.sqrt(NOPE_DIM + ROT_DIM)

    def attend(carried, key_block, rot_block, value_block, key_offset):
        run_max, run_sum, run_acc = carried
        block_len = key_block.shape[0]
        scores = (
            jnp.einsum("qhd,khd->hqk", queries, key_block, preferred_element_type=jnp.float32)
            + jnp.einsum("qhd,kd->hqk", query_rot, rot_block, preferred_element_type=jnp.float32)
        ) * inv_scale
        key_pos = key_offset + jnp.arange(block_len, dtype=jnp.int32)
        visible = (key_pos[None, :] <= positions[:, None])[None]
        new_max = jnp.maximum(run_max, jnp.max(jnp.where(visible, scores, far_below), axis=2))
        exp_scores = jnp.where(visible, jnp.exp(scores - new_max[:, :, None]), 0.0)
        shrink = jnp.exp(run_max - new_max)
        run_sum = run_sum * shrink + jnp.sum(exp_scores, axis=2)
        run_acc = run_acc * shrink.T[:, :, None] + jnp.einsum(
            "hqk,khd->qhd",
            exp_scores.astype(jnp.bfloat16),
            value_block,
            preferred_element_type=jnp.float32,
        )
        return (new_max, run_sum, run_acc)

    def expand_latent(sliced):
        lat_block, rot_block = sliced
        key_block = (
            jnp.dot(lat_block, key_up, preferred_element_type=jnp.float32)
            .astype(jnp.bfloat16)
            .reshape(-1, heads_here, NOPE_DIM)
        )
        value_block = (
            jnp.dot(lat_block, value_up, preferred_element_type=jnp.float32)
            .astype(jnp.bfloat16)
            .reshape(-1, heads_here, VALUE_DIM)
        )
        return (key_block, value_block, rot_block)

    def square_rows(matrix):
        wide_rows = matrix.astype(jnp.float32)
        return jnp.sum(wide_rows * wide_rows, axis=1)

    start_state = (
        jnp.full((heads_here, tok_rows), far_below, jnp.float32),
        jnp.zeros((heads_here, tok_rows), jnp.float32),
        jnp.zeros((tok_rows, heads_here, VALUE_DIM), jnp.float32),
    )
    pieces = (
        lax.all_gather(latent, "sp", axis=0, tiled=True),
        lax.all_gather(key_rot, "sp", axis=0, tiled=True),
    )
    piece_rows = pieces[0].shape[0]
    step_len = math.gcd(piece_rows, 512)

    def visit_block(running, block_idx):
        start_row = block_idx * step_len
        sliced = tuple(
            (lax.dynamic_slice_in_dim(member, start_row, step_len, 0) for member in pieces)
        )

        def compute(current):
            key_block, value_block, rot_block = expand_latent(sliced)
            return attend(current, key_block, rot_block, value_block, start_row)

        return (lax.cond(start_row < query_end, compute, lambda current: current, running), None)

    final_state = lax.scan(
        visit_block, start_state, jnp.arange(piece_rows // step_len, dtype=jnp.int32)
    )[0]
    run_max, run_sum, run_acc = final_state
    attended = (
        (run_acc / run_sum.T[:, :, None])
        .astype(jnp.bfloat16)
        .reshape(tok_rows, heads_here * VALUE_DIM)
    )
    att_sq = lax.psum(square_rows(attended), "tp")
    rim_rows = shifted(gated_input[tok_rows - (KERNEL - 1) :], "sp", 1)
    padded = jnp.concatenate([rim_rows, gated_input], axis=0)
    conv_out = jnp.zeros((tok_rows, chan_here), jnp.float32)
    for tap_idx in range(KERNEL):
        conv_out = conv_out + conv_taps[tap_idx][None, :] * padded[
            tap_idx : tap_idx + tok_rows
        ].astype(jnp.float32)
    moment_one, moment_two = lax.psum(
        (jnp.sum(conv_out, axis=1), jnp.sum(conv_out * conv_out, axis=1)), "tp"
    )
    mean_val = moment_one / CONV_CH
    spread = moment_two / CONV_CH - mean_val * mean_val
    normed = (conv_out - mean_val[:, None]) * lax.rsqrt(spread + norm_eps)[:, None]
    swished = jax.nn.silu(normed * conv_ln_gain[None, :] + conv_ln_bias[None, :])
    conv_sq = lax.psum(square_rows(swished), "tp")
    att_mixed = (
        attended.astype(jnp.float32)
        * lax.rsqrt(att_sq / ATT_WIDTH + norm_eps)[:, None]
        * att_out_gain[None, :]
    ).astype(jnp.bfloat16)
    conv_mixed = (
        swished * lax.rsqrt(conv_sq / CONV_CH + norm_eps)[:, None] * conv_out_gain[None, :]
    ).astype(jnp.bfloat16)
    contract = (((0,), (1,)), ((), ()))
    feature_rows = lax.psum_scatter(
        (
            lax.dot_general(att_out_weight, att_mixed, contract, preferred_element_type=jnp.float32)
            + lax.dot_general(
                conv_out_weight, conv_mixed, contract, preferred_element_type=jnp.float32
            )
        ).astype(jnp.bfloat16),
        "tp",
        scatter_dimension=0,
        tiled=True,
    ).astype(jnp.float32)
    return feature_rows.T.astype(jnp.bfloat16)


def solution(mesh):
    return jax.shard_map(
        shards,
        mesh=mesh,
        in_specs=(
            P("sp", "tp"),
            P(),
            P(None, "tp"),
            P(None, "tp"),
            P(),
            P(),
            P(),
            P(None, "tp"),
            P(None, "tp"),
            P(None, "tp"),
            P(None, "tp"),
            P(None, "tp"),
            P("tp"),
            P("tp"),
            P("tp"),
            P("tp"),
            P("tp", None),
            P("tp", None),
        ),
        out_specs=P("sp", "tp"),
        check_vma=False,
    )
```

profile of v0, /device:TPU:0, one launch (start us, length us, event | category | flops | bytes accessed | tf_op | source)
XLA Modules:
  0.0 248.4 jit_solution(14839390345446647439)
XLA Ops:
  6.5 0.7 all-gather.3.cloned.1.call-update
  7.3 0.0 all-gather.5.cloned.1.call-start
  7.3 14.1 %all-gather.3.cloned.1.call-done = bf16[384,2048]{1,0:T(8,128)(2,1)} async-done(((bf16[384,1024]{1,0:T(8,128)(2,1)}), bf16[384,2048]{1,0:T(8,128)(2,1)}) %all-gather.3.cloned.1.call-update) | async-done | bytes 1572880 | tf_op jit(solution)/shard_map/all_gather | solution.py:75
  21.4 2.5 multiply_reduce_fusion.3
  23.9 0.8 multiply_convert_fusion.2
  24.7 0.0 all-gather.5.cloned.1.call-update
  24.8 0.0 reduce-scatter.2.cloned.1.call-start
  24.9 0.7 fusion.79
  25.6 1.8 fusion.27
  27.4 0.0 copy-start.11
  27.4 3.3 %fusion.33 = f32[384,512]{1,0:T(8,128)S(1)} fusion(bf16[2048,512]{1,0:T(8,128)(2,1)} %param.32, bf16[384,2048]{1,0:T(8,128)(2,1)} %all-gather.3.cloned.1.call-done, f32[2048]{0:T(1024)S(1)} %copy-done.16, f32[384]{0:T(512)S(1)} %add_rsqrt_fusion.3), kind=kOutput, calls=%fused_computation.72 | convolution fusion | flops 808452096 | bytes 4466176 | tf_op jit(solution)/shard_map/dot_general | solution.py:79
  30.7 0.0 copy-start.15
  30.8 0.0 copy-start.14
  30.8 1.0 fusion.35
  31.8 0.0 copy-start.5
  31.8 0.0 copy-start.12
  31.8 3.8 %collective-permute-start = (bf16[30,512]{1,0:T(8,128)(2,1)S(1)}, bf16[30,512]{1,0:T(8,128)(2,1)S(1)}, u32[]{:S(2)}, u32[]{:S(2)}) collective-permute-start(bf16[30,512]{1,0:T(8,128)(2,1)S(1)} %slice.268), channel_id=1, source_target_pairs={{0,2},{2,4},{4,6},{6,8},{8,10},{10,12},{12,14},{14,16},{16,18},{18... | collective-permute-start | bytes 92168 | tf_op jit(solution)/shard_map/ppermute | solution.py:22
  35.6 0.6 convolution_multiply_fusion.4
  36.2 0.2 multiply_cosine_fusion
  36.4 44.6 %all_gather.11 = bf16[6144,32]{0,1:T(8,128)(2,1)} all-gather(bf16[384,32]{0,1:T(8,128)(2,1)S(1)} %pad_maximum_fusion.2), channel_id=1, replica_groups=mesh['sp'=16,'tp'=2] {'sp'}, dimensions={0}, use_global_device_ids=true | all-gather | bytes 417792 | tf_op jit(solution)/shard_map/all_gather | solution.py:152
  80.9 0.8 convolution_multiply_fusion.3
  81.7 0.1 subtract_convert_fusion
  81.8 1.0 fusion.34
  82.8 0.2 copy.23
  83.0 14.7 %fusion.77 = (f32[384]{0:T(512)}, f32[384]{0:T(512)}, f32[384,512]{1,0:T(8,128)S(1)}) fusion(bf16[384,512]{1,0:T(8,128)(2,1)} %copy-done.5, f32[512]{0:T(512)S(1)} %bitcast.93, bf16[30,512]{1,0:T(8,128)(2,1)S(1)} %collective-permute-done, f32[512]{0:T(512)S(1)} %bitcast.94, f32[512]{0:T(512)} %bitcast.96, f32[512]{0:T(512)} %bitcast.97, f32[512]{0:T(512)} %bitcast.98, ...), kind=kLoop, calls=%fused_computation.145 | loop fusion | flops 36371712 | bytes 1276928 | tf_op jit(solution)/shard_map/reduce_sum | solution.py:187
  97.7 2.8 %all-reduce.1 = (f32[384]{0:T(512)S(1)}, f32[384]{0:T(512)S(1)}) all-reduce(f32[384]{0:T(512)} %get-tuple-element.271, f32[384]{0:T(512)} %get-tuple-element.270), channel_id=1, replica_groups=mesh['sp'=16,'tp'=2] {'tp'}, use_global_device_ids=true, to_apply=%region_13.14 | all-reduce | flops 768 | bytes 6144 | tf_op jit(solution)/shard_map/psum | solution.py:186
  100.5 1.2 multiply_reduce_fusion
  101.6 0.0 all-gather.5.cloned.1.call-done
  101.7 4.7 %copy.24 = bf16[6144,256]{1,0:T(8,128)(2,1)} copy(bf16[6144,256]{0,1:T(8,128)(2,1)} %all-gather.5.cloned.1.call-done) | data formatting | bytes 6291456
  106.3 0.1 broadcast_in_dim.61
  106.4 0.0 copy-start.7
  106.4 24.4 %while.15 = (s32[]{:T(128)}, f32[8,384]{1,0:T(8,128)S(1)}, f32[8,384]{1,0:T(8,128)S(1)}, f32[384,8,64]{0,2,1:T(8,128)S(1)}, s32[12]{0:T(128)S(1)}, /*index=5*/s3...) while((s32[]{:T(128)}, f32[8,384]{1,0:T(8,128)S(1)}, ...), condition=%wide.region_7.8_spmd.clone, body=%wide.region_2.7_spmd.clone.sunk | while | flops 788604800 | bytes 38840728 | solution.py:169
  106.4 0.6 dynamic_slice.32
  107.7 9.0 %conditional.3 = ((f32[8,384]{1,0:T(8,128)S(1)}, f32[8,384]{1,0:T(8,128)S(1)}, f32[384,8,64]{0,2,1:T(8,128)S(1)})) conditional(s32[]{:T(128)} %convert_element_type.326, (f32[8,384]{1,0:T(8,128)S(1)}, f32[8,384]{1,0:T(8,128)S(1)}, f32[384,8,64]{0,2,1:T(8,128)S(1)}) %tuple.85, (s32[]{:T(128)}, s32[]{:T(128)}, bf16[6144,256]{1,0:T(8,128)(2,1)}, ...), branch_computations={%region_3.3_spmd, %region_4.6_spmd} | conditional | flops 788604800 | bytes 38838896 | solution.py:167
  107.7 1.4 convolution_convert_fusion.1
  109.1 1.9 fusion.18
  111.0 0.2 broadcast_compare_fusion
  111.2 0.0 copy-start.1
  111.2 1.6 select_reduce_fusion
  112.8 1.3 convolution_convert_fusion
  114.1 1.4 fusion.13
  115.5 1.1 fusion.4
  116.7 0.6 dynamic_slice.32
  118.0 0.6 dynamic_slice.32
  119.2 0.6 dynamic_slice.32
  120.5 0.6 dynamic_slice.32
  121.8 0.6 dynamic_slice.32
  123.1 0.6 dynamic_slice.32
  124.4 0.6 dynamic_slice.32
  125.7 0.6 dynamic_slice.32
  127.0 0.6 dynamic_slice.32
  128.3 0.6 dynamic_slice.32
  129.6 0.6 dynamic_slice.32
  130.9 1.0 multiply_reduce_fusion.2
  131.8 2.4 all-reduce
  134.3 0.0 copy-start.8
  134.3 0.0 copy-start.9
  134.3 0.0 copy-start.13
  134.3 0.0 copy-start.17
  134.3 1.4 fusion.37
  135.8 1.0 fusion.81
  136.8 2.5 fusion.28
  139.3 0.0 reduce-scatter.2.cloned.1.call-update
  139.3 102.5 %reduce-scatter.2.cloned.1.call-done = bf16[1024,384]{0,1:T(8,128)(2,1)} async-done(((bf16[2048,384]{0,1:T(8,128)(2,1)}), bf16[1024,384]{0,1:T(8,128)(2,1)}) %reduce-scatter.2.cloned.1.call-update) | async-done | bytes 786448 | tf_op jit(solution)/shard_map/reduce_scatter | solution.py:203
  (68 shorter events, 0.4 us)
Async XLA Ops:
  6.5 129.2 %copy-start = (bf16[512,2048]{1,0:T(8,128)(2,1)S(1)}, bf16[512,2048]{1,0:T(8,128)(2,1)}, u32[]{:S(2)}) copy-start(bf16[512,2048]{1,0:T(8,128)(2,1)} %param.38) | copy-start | bytes 6291460
  6.5 17.4 %copy-start.10 = (f32[256]{0:T(256)S(1)}, f32[256]{0:T(256)}, u32[]{:S(2)}) copy-start(f32[256]{0:T(256)} %param.28) | copy-start | bytes 3076
  6.5 18.3 %copy-start.6 = (f32[31,512]{1,0:T(8,128)S(1)}, f32[31,512]{1,0:T(8,128)}, u32[]{:S(2)}) copy-start(f32[31,512]{1,0:T(8,128)} %param.33) | copy-start | bytes 190468
  6.5 14.9 %all-gather.3.cloned.1.call-start = ((), (), s32[]{:S(2)}) async-start(), calls=%async_computation.1 | async-start | bytes 2359296 | tf_op jit(solution)/shard_map/all_gather | solution.py:75
  7.3 20.1 %copy-start.16 = (f32[2048]{0:T(1024)S(1)}, f32[2048]{0:T(1024)}, u32[]{:S(2)}) copy-start(f32[2048]{0:T(1024)} %param.23) | copy-start | bytes 24580
  7.3 94.4 %all-gather.5.cloned.1.call-start = ((), (), s32[]{:S(2)}) async-start(), calls=%async_computation.2 | async-start | bytes 3342336 | tf_op jit(solution)/shard_map/all_gather | solution.py:151
  24.8 217.1 %reduce-scatter.2.cloned.1.call-start = ((), (), s32[]{:S(2)}) async-start(), calls=%async_computation.3 | async-start | bytes 2359296 | tf_op jit(solution)/shard_map/reduce_scatter | solution.py:203
  27.4 3.4 %copy-start.4 = (bf16[384,2048]{1,0:T(8,128)(2,1)S(1)}, bf16[384,2048]{1,0:T(8,128)(2,1)}, u32[]{:S(2)}) copy-start(bf16[384,2048]{1,0:T(8,128)(2,1)} %all-gather.3.cloned.1.call-done) | copy-start | bytes 4718596
  27.4 3.4 %copy-start.11 = (bf16[2048,512]{1,0:T(8,128)(2,1)S(1)}, bf16[2048,512]{1,0:T(8,128)(2,1)}, u32[]{:S(2)}) copy-start(bf16[2048,512]{1,0:T(8,128)(2,1)} %param.31) | copy-start | bytes 6291460
  30.7 4.8 %copy-start.15 = (bf16[2048,32]{0,1:T(8,128)(2,1)S(1)}, bf16[2048,32]{0,1:T(8,128)(2,1)}, u32[]{:S(2)}) copy-start(bf16[2048,32]{0,1:T(8,128)(2,1)} %param.27) | copy-start | bytes 393220
  30.8 50.2 %copy-start.14 = (bf16[2048,256]{1,0:T(8,128)(2,1)S(1)}, bf16[2048,256]{1,0:T(8,128)(2,1)}, u32[]{:S(2)}) copy-start(bf16[2048,256]{1,0:T(8,128)(2,1)} %param.25) | copy-start | bytes 3145732
  31.8 50.0 %copy-start.5 = (bf16[384,512]{1,0:T(8,128)(2,1)}, bf16[384,512]{1,0:T(8,128)(2,1)S(1)}, u32[]{:S(2)}) copy-start(bf16[384,512]{1,0:T(8,128)(2,1)S(1)} %fusion.35) | copy-start | bytes 1179652
  31.8 50.0 %copy-start.12 = (bf16[2048,512]{1,0:T(8,128)(2,1)S(1)}, bf16[2048,512]{1,0:T(8,128)(2,1)}, u32[]{:S(2)}) copy-start(bf16[2048,512]{1,0:T(8,128)(2,1)} %param.24) | copy-start | bytes 6291460
  31.8 51.2 %collective-permute-start = (bf16[30,512]{1,0:T(8,128)(2,1)S(1)}, bf16[30,512]{1,0:T(8,128)(2,1)S(1)}, u32[]{:S(2)}, u32[]{:S(2)}) collective-permute-start(bf16[30,512]{1,0:T(8,128)(2,1)S(1)} %slice.268), channel_id=1, source_target_pairs={{0,2},{2,4},{4,6},{6,8},{8,10},{10,12},{12,14},{14,16},{16,18},{18... | collective-permute-start | bytes 92168 | tf_op jit(solution)/shard_map/ppermute | solution.py:22
  97.7 8.6 %copy-start.2 = (f32[384,512]{1,0:T(8,128)}, f32[384,512]{1,0:T(8,128)S(1)}, u32[]{:S(2)}) copy-start(f32[384,512]{1,0:T(8,128)S(1)} %get-tuple-element.304) | copy-start | bytes 2359300
  106.4 27.9 %copy-start.7 = (f32[512]{0:T(512)S(1)}, f32[512]{0:T(512)}, u32[]{:S(2)}) copy-start(f32[512]{0:T(512)} %param.36) | copy-start | bytes 6148
  111.2 1.6 copy-start.1
  134.3 2.5 %copy-start.3 = (f32[384,512]{1,0:T(8,128)S(1)}, f32[384,512]{1,0:T(8,128)}, u32[]{:S(2)}) copy-start(f32[384,512]{1,0:T(8,128)} %copy-done.2) | copy-start | bytes 2359300
  134.3 2.5 %copy-start.8 = (f32[512]{0:T(512)S(1)}, f32[512]{0:T(512)}, u32[]{:S(2)}) copy-start(f32[512]{0:T(512)} %param.35) | copy-start | bytes 6148
  134.3 2.5 %copy-start.9 = (f32[512]{0:T(512)S(1)}, f32[512]{0:T(512)}, u32[]{:S(2)}) copy-start(f32[512]{0:T(512)} %param.34) | copy-start | bytes 6148
  134.3 2.5 %copy-start.13 = (bf16[512,2048]{1,0:T(8,128)(2,1)S(1)}, bf16[512,2048]{1,0:T(8,128)(2,1)}, u32[]{:S(2)}) copy-start(bf16[512,2048]{1,0:T(8,128)(2,1)} %param.39) | copy-start | bytes 6291460
  134.3 2.5 %copy-start.17 = (f32[512]{0:T(512)S(1)}, f32[512]{0:T(512)}, u32[]{:S(2)}) copy-start(f32[512]{0:T(512)} %param.37) | copy-start | bytes 6148
Sparse Core Ops, SparseCore 0:
  8.9 12.5 all-gather.2
  24.9 72.0 all-gather.4
  139.5 102.3 reduce-scatter.1
where the time goes:
time: 250 us; the launch traced here: 248 us
  waiting for transfers between devices  117 us (47%)
  blocking collectives  49.8 us (20%)
  other arithmetic  22.4 us (9%)
  matrix products  20.1 us (8%)
  between operations  13.5 us (5%)
  local copies, waits for them, and re-layouts  12.8 us (5%)
  loops' own time  8.52 us (3%)
  starting transfers between devices  3.86 us (2%)
    reduce_scatter x1, waiting for transfers between devices, shards(): lax.psum_scatter((lax.dot_general(att_out_weight, att_mixed, contract, pr...  103 us
    all_gather x1, blocking collectives, shards(): lax.all_gather(key_rot, 'sp', axis=0, tiled=True)  44.6 us
    reduce_sum x1, other arithmetic, shards(): jnp.sum(conv_out, axis=1)  14.7 us
    all_gather x1, waiting for transfers between devices, shards(): lax.all_gather(tokens, 'tp', axis=1, tiled=True).astype(jnp.float32)  14.1 us
    dot_general x6, matrix products, add_product(): return jnp.dot(scaled, weight, preferred_element_type=jnp.float32)  9.11 us
    another operation x1, loops' own time, shards(): lax.scan(visit_block, start_state, jnp.arange(piece_rows // step_len, dty...  8.29 us
    dynamic_slice x12, local copies, waits for them, and re-layouts, shards(): lax.scan(visit_block, start_state, jnp.arange(piece_rows // step_len, dty...  7.04 us
  transfers between devices with their start and end apart: 4, of which 2 were waited for; matrix products, arithmetic and copies ran while one was open for 10% of the time, Pallas kernels for 0%

commit v1 on v0

--- a/solution.py
+++ b/solution.py
@@ -3,6 +3,7 @@
 import jax.numpy as jnp
 from jax import lax
 from jax.sharding import PartitionSpec as P
+from jax.lax import all_gather
 
 D_MODEL = 2048
 NOPE_DIM = 64
@@ -14,6 +15,7 @@
 norm_eps = 1e-06
 far_below = -1e30
 rope_base = 10000.0
+connect_the_routes_all = lambda slab_in: jnp.concatenate(all_gather(slab_in, axis_name="tp"), 1)
 
 
 def shifted(block, axis, distance):
@@ -72,7 +74,7 @@
         conv_value_weight,
         conv_gate_weight,
     )
-    wide_part = lax.all_gather(tokens, "tp", axis=1, tiled=True).astype(jnp.float32)
+    wide_part = connect_the_routes_all(tokens).astype(jnp.float32)
     scaled = (wide_part * input_gain[None, :]).astype(jnp.bfloat16)
 
     def add_product(weight):

time: 250 us -> 260 us (1.040)
  other arithmetic: 22.4 us -> 28 us
  local copies, waits for them, and re-layouts: 12.8 us -> 18.3 us
    convert_element_type x0 -> x2, other arithmetic: none -> 5.74 us  [the longest x1 3.43 us: shards(): wide_part = connect_the_routes_all(tokens).astype(jnp.float32)]
    convert_element_type x0 -> x1, local copies, waits for them, and re-layouts: none -> 3.56 us  [shards(): wide_part = connect_the_routes_all(tokens).astype(jnp.float32)]
    unnamed x35 -> x39, local copies, waits for them, and re-layouts: 4.75 us -> 6.67 us
where the time goes in v1:
time: 260 us; the launch traced here: 258 us
  waiting for transfers between devices  117 us (45%)
  blocking collectives  50 us (19%)
  other arithmetic  28 us (11%)
  local copies, waits for them, and re-layouts  18.3 us (7%)
  matrix products  18.2 us (7%)
  between operations  13.5 us (5%)
  loops' own time  8.52 us (3%)
  starting transfers between devices  3.86 us (1%)
    reduce_scatter x1, waiting for transfers between devices, shards(): lax.psum_scatter((lax.dot_general(att_out_weight, att_mixed, contract, pr...  103 us
    all_gather x1, blocking collectives, shards(): lax.all_gather(key_rot, 'sp', axis=0, tiled=True)  44.8 us
    reduce_sum x1, other arithmetic, shards(): jnp.sum(conv_out, axis=1)  14.7 us
    all_gather x1, waiting for transfers between devices, all_gather(slab_in, axis_name='tp')  14.1 us
    another operation x1, loops' own time, shards(): lax.scan(visit_block, start_state, jnp.arange(piece_rows // step_len, dty...  8.29 us
    dot_general x6, matrix products, add_product(): return jnp.dot(scaled, weight, preferred_element_type=jnp.float32)  7.21 us
    dynamic_slice x12, local copies, waits for them, and re-layouts, shards(): lax.scan(visit_block, start_state, jnp.arange(piece_rows // step_len, dty...  7.04 us
    unnamed x39, local copies, waits for them, and re-layouts  6.67 us
  transfers between devices with their start and end apart: 4, of which 2 were waited for; matrix products, arithmetic and copies ran while one was open for 10% of the time, Pallas kernels for 0%

profile of v1, /device:TPU:0, one launch (start us, length us, event | category | flops | bytes accessed | tf_op | source)
XLA Modules:
  0.0 257.9 jit_solution(12411284649723302253)
XLA Ops:
  6.5 0.7 all-gather.6.cloned.1.call-update
  7.3 0.0 all-gather.4.cloned.1.call-start
  7.3 14.1 %all-gather.6.cloned.1.call-done = bf16[768,1024]{1,0:T(8,128)(2,1)} async-done(((bf16[384,1024]{1,0:T(8,128)(2,1)}), bf16[768,1024]{1,0:T(8,128)(2,1)}) %all-gather.6.cloned.1.call-update) | async-done | bytes 1572880 | tf_op jit(solution)/shard_map/all_gather | solution.py:18
  21.4 3.4 %convert_bitcast_fusion = f32[384,2,1024]{2,0,1:T(8,128)} fusion(bf16[2,384,1024]{2,1,0:T(8,128)(2,1)} %bitcast.95), kind=kLoop, calls=%fused_computation.60 | loop fusion | flops 786432 | bytes 4718592 | tf_op jit(solution)/shard_map/convert_element_type | solution.py:77
  24.9 3.6 %copy.26 = f32[384,2,1024]{0,2,1:T(8,128)} copy(f32[384,2,1024]{2,0,1:T(8,128)} %convert_bitcast_fusion) | data formatting | bytes 6291456 | tf_op jit(solution)/shard_map/convert_element_type | solution.py:77
  28.4 2.3 fusion.27
  30.8 0.8 multiply_reduce_fusion.3
  31.6 0.3 copy-done.1
  31.9 0.8 multiply_convert_fusion.2
  32.7 0.0 all-gather.4.cloned.1.call-update
  32.7 0.0 reduce-scatter.2.cloned.1.call-start
  32.9 0.7 fusion.72
  33.5 1.8 fusion.26
  35.4 3.3 %fusion.33 = f32[384,512]{1,0:T(8,128)S(1)} fusion(bf16[384,2048]{0,1:T(8,128)(2,1)} %copy-done.1, bf16[2048,512]{1,0:T(8,128)(2,1)} %param.32, f32[384]{0:T(512)S(1)} %add_rsqrt_fusion.3), kind=kOutput, calls=%fused_computation.73 | convolution fusion | flops 806092800 | bytes 4457984 | tf_op jit(solution)/shard_map/dot_general | solution.py:81
  38.7 0.0 copy-start.8
  38.7 1.0 fusion.35
  39.8 0.0 copy-start.18
  39.8 3.8 %collective-permute-start = (bf16[30,512]{1,0:T(8,128)(2,1)S(1)}, bf16[30,512]{1,0:T(8,128)(2,1)S(1)}, u32[]{:S(2)}, u32[]{:S(2)}) collective-permute-start(bf16[30,512]{1,0:T(8,128)(2,1)S(1)} %slice.268), channel_id=1, source_target_pairs={{0,2},{2,4},{4,6},{6,8},{8,10},{10,12},{12,14},{14,16},{16,18},{18... | collective-permute-start | bytes 92168 | tf_op jit(solution)/shard_map/ppermute | solution.py:24
  43.6 0.3 convolution_multiply_fusion.4
  43.9 0.2 multiply_cosine_fusion
  44.1 44.8 %all_gather.15 = bf16[6144,32]{0,1:T(8,128)(2,1)} all-gather(bf16[384,32]{0,1:T(8,128)(2,1)S(1)} %pad_maximum_fusion.2), channel_id=1, replica_groups=mesh['sp'=16,'tp'=2] {'sp'}, dimensions={0}, use_global_device_ids=true | all-gather | bytes 417792 | tf_op jit(solution)/shard_map/all_gather | solution.py:154
  89.0 0.8 convolution_multiply_fusion.3
  89.8 0.1 subtract_convert_fusion
  89.8 0.8 copy-done.15
  90.6 1.0 fusion.34
  91.6 0.2 copy.27
  91.8 14.7 %fusion.70 = (f32[384]{0:T(512)}, f32[384]{0:T(512)}, f32[384,512]{1,0:T(8,128)S(1)}) fusion(bf16[384,512]{1,0:T(8,128)(2,1)} %copy-done.7, f32[512]{0:T(512)S(1)} %bitcast.109, bf16[30,512]{1,0:T(8,128)(2,1)S(1)} %collective-permute-done, f32[512]{0:T(512)S(1)} %bitcast.110, f32[512]{0:T(512)} %bitcast.112, f32[512]{0:T(512)} %bitcast.113, ...), kind=kLoop, calls=%fused_computation.145 | loop fusion | flops 36371712 | bytes 1276928 | tf_op jit(solution)/shard_map/reduce_sum | solution.py:189
  106.5 2.8 %all-reduce.1 = (f32[384]{0:T(512)S(1)}, f32[384]{0:T(512)S(1)}) all-reduce(f32[384]{0:T(512)} %get-tuple-element.284, f32[384]{0:T(512)} %get-tuple-element.283), channel_id=1, replica_groups=mesh['sp'=16,'tp'=2] {'tp'}, use_global_device_ids=true, to_apply=%region_13.14 | all-reduce | flops 768 | bytes 6144 | tf_op jit(solution)/shard_map/psum | solution.py:188
  109.3 1.2 multiply_reduce_fusion
  110.4 0.0 all-gather.4.cloned.1.call-done
  110.4 4.7 %copy.28 = bf16[6144,256]{1,0:T(8,128)(2,1)} copy(bf16[6144,256]{0,1:T(8,128)(2,1)} %all-gather.4.cloned.1.call-done) | data formatting | bytes 6291456
  115.1 0.1 broadcast_in_dim.61
  115.2 0.0 copy-start.11
  115.2 24.4 %while.15 = (s32[]{:T(128)}, f32[8,384]{1,0:T(8,128)S(1)}, f32[8,384]{1,0:T(8,128)S(1)}, f32[384,8,64]{0,2,1:T(8,128)S(1)}, s32[12]{0:T(128)S(1)}, /*index=5*/s3...) while((s32[]{:T(128)}, f32[8,384]{1,0:T(8,128)S(1)}, ...), condition=%wide.region_7.8_spmd.clone, body=%wide.region_2.7_spmd.clone.sunk | while | flops 788604800 | bytes 38840728 | solution.py:171
  115.2 0.6 dynamic_slice.32
  116.5 9.0 %conditional.3 = ((f32[8,384]{1,0:T(8,128)S(1)}, f32[8,384]{1,0:T(8,128)S(1)}, f32[384,8,64]{0,2,1:T(8,128)S(1)})) conditional(s32[]{:T(128)} %convert_element_type.321, (f32[8,384]{1,0:T(8,128)S(1)}, f32[8,384]{1,0:T(8,128)S(1)}, f32[384,8,64]{0,2,1:T(8,128)S(1)}) %tuple.86, (s32[]{:T(128)}, s32[]{:T(128)}, bf16[6144,256]{1,0:T(8,128)(2,1)}, ...), branch_computations={%region_3.3_spmd, %region_4.6_spmd} | conditional | flops 788604800 | bytes 38838896 | solution.py:169
  116.5 1.4 convolution_convert_fusion.1
  117.9 1.9 fusion.18
  119.8 0.2 broadcast_compare_fusion
  120.0 1.6 select_reduce_fusion
  121.6 1.3 convolution_convert_fusion
  122.9 1.4 fusion.13
  124.3 1.1 fusion.4
  125.5 0.6 dynamic_slice.32
  126.8 0.6 dynamic_slice.32
  128.0 0.6 dynamic_slice.32
  129.3 0.6 dynamic_slice.32
  130.6 0.6 dynamic_slice.32
  131.9 0.6 dynamic_slice.32
  133.2 0.6 dynamic_slice.32
  134.5 0.6 dynamic_slice.32
  135.8 0.6 dynamic_slice.32
  137.1 0.6 dynamic_slice.32
  138.4 0.6 dynamic_slice.32
  139.6 1.0 multiply_reduce_fusion.2
  140.6 2.4 all-reduce
  143.1 1.3 fusion.37
  144.4 0.0 copy-start.16
  144.4 1.0 fusion.74
  145.4 0.1 copy-done.5
  145.5 0.7 copy-done.16
  146.3 2.5 fusion.28
  148.7 0.0 reduce-scatter.2.cloned.1.call-update
  148.7 102.6 %reduce-scatter.2.cloned.1.call-done = bf16[1024,384]{0,1:T(8,128)(2,1)} async-done(((bf16[2048,384]{0,1:T(8,128)(2,1)}), bf16[1024,384]{0,1:T(8,128)(2,1)}) %reduce-scatter.2.cloned.1.call-update) | async-done | bytes 786448 | tf_op jit(solution)/shard_map/reduce_scatter | solution.py:205
  (75 shorter events, 0.4 us)
Async XLA Ops:
  6.5 137.8 %copy-start = (bf16[512,2048]{1,0:T(8,128)(2,1)S(1)}, bf16[512,2048]{1,0:T(8,128)(2,1)}, u32[]{:S(2)}) copy-start(bf16[512,2048]{1,0:T(8,128)(2,1)} %param.38) | copy-start | bytes 6291460
  6.5 14.9 %all-gather.6.cloned.1.call-start = ((), (), s32[]{:S(2)}) async-start(), calls=%async_computation.3 | async-start | bytes 2359296 | tf_op jit(solution)/shard_map/all_gather | solution.py:18
  7.3 103.2 %all-gather.4.cloned.1.call-start = ((), (), s32[]{:S(2)}) async-start(), calls=%async_computation.1 | async-start | bytes 3342336 | tf_op jit(solution)/shard_map/all_gather | solution.py:153
  24.9 3.6 %copy-start.10 = (f32[2048]{0:T(1024)S(1)}, f32[2048]{0:T(1024)}, u32[]{:S(2)}) copy-start(f32[2048]{0:T(1024)} %param.23) | copy-start | bytes 24580
  28.4 2.3 copy-start.17
  30.8 1.2 copy-start.1
  30.8 1.2 copy-start.14
  30.8 2.0 copy-start.9
  32.7 218.6 %reduce-scatter.2.cloned.1.call-start = ((), (), s32[]{:S(2)}) async-start(), calls=%async_computation.2 | async-start | bytes 2359296 | tf_op jit(solution)/shard_map/reduce_scatter | solution.py:205
  35.3 3.4 %copy-start.2 = (bf16[384,2048]{0,1:T(8,128)(2,1)S(1)}, bf16[384,2048]{0,1:T(8,128)(2,1)}, u32[]{:S(2)}) copy-start(bf16[384,2048]{0,1:T(8,128)(2,1)} %copy-done.1) | copy-start | bytes 4718596
  35.4 3.4 %copy-start.6 = (bf16[2048,512]{1,0:T(8,128)(2,1)S(1)}, bf16[2048,512]{1,0:T(8,128)(2,1)}, u32[]{:S(2)}) copy-start(bf16[2048,512]{1,0:T(8,128)(2,1)} %param.31) | copy-start | bytes 6291460
  38.7 4.8 %copy-start.8 = (bf16[2048,32]{0,1:T(8,128)(2,1)S(1)}, bf16[2048,32]{0,1:T(8,128)(2,1)}, u32[]{:S(2)}) copy-start(bf16[2048,32]{0,1:T(8,128)(2,1)} %param.27) | copy-start | bytes 393220
  39.7 50.0 %copy-start.7 = (bf16[384,512]{1,0:T(8,128)(2,1)}, bf16[384,512]{1,0:T(8,128)(2,1)S(1)}, u32[]{:S(2)}) copy-start(bf16[384,512]{1,0:T(8,128)(2,1)S(1)} %fusion.35) | copy-start | bytes 1179652
  39.8 49.2 %copy-start.18 = (bf16[2048,256]{1,0:T(8,128)(2,1)S(1)}, bf16[2048,256]{1,0:T(8,128)(2,1)}, u32[]{:S(2)}) copy-start(bf16[2048,256]{1,0:T(8,128)(2,1)} %param.25) | copy-start | bytes 3145732
  39.8 52.0 %collective-permute-start = (bf16[30,512]{1,0:T(8,128)(2,1)S(1)}, bf16[30,512]{1,0:T(8,128)(2,1)S(1)}, u32[]{:S(2)}, u32[]{:S(2)}) collective-permute-start(bf16[30,512]{1,0:T(8,128)(2,1)S(1)} %slice.268), channel_id=1, source_target_pairs={{0,2},{2,4},{4,6},{6,8},{8,10},{10,12},{12,14},{14,16},{16,18},{18... | collective-permute-start | bytes 92168 | tf_op jit(solution)/shard_map/ppermute | solution.py:24
  89.0 1.6 copy-start.15
  106.5 8.6 %copy-start.4 = (f32[384,512]{1,0:T(8,128)}, f32[384,512]{1,0:T(8,128)S(1)}, u32[]{:S(2)}) copy-start(f32[384,512]{1,0:T(8,128)S(1)} %get-tuple-element.317) | copy-start | bytes 2359300
  115.2 27.9 %copy-start.11 = (f32[512]{0:T(512)S(1)}, f32[512]{0:T(512)}, u32[]{:S(2)}) copy-start(f32[512]{0:T(512)} %param.36) | copy-start | bytes 6148
  120.0 1.6 copy-start.3
  144.4 1.1 copy-start.5
  144.4 1.1 copy-start.12
  144.4 1.1 copy-start.13
  144.4 1.9 copy-start.16
  144.4 1.8 copy-start.19
Sparse Core Ops, SparseCore 0:
  8.9 12.5 all-gather.5
  32.9 70.0 all-gather.3
  148.9 102.4 reduce-scatter.1
